TPU v7x, 256 devices: a whole 4x4x8 slice. The times are simulated.
256 devices in a mesh: ep: 32 (over z, x), tp: 8 (over y, core).
Axes of the slice: x: 4, y: 4, z: 8, core: 2. Of those that a mesh axis runs over, the one named last changes fastest.
Arguments:
- resid: bfloat16 [1024, 2048], P('ep'), may hold values from -6 to 6
- norm_gain: bfloat16 [2048], replicated, may hold values from 0.099609375 to 1.8984375
- w_query: bfloat16 [2048, 1024], P(None, 'tp'), may hold values from -0.125 to 0.125
- w_key: bfloat16 [2048, 1024], P(None, 'tp'), may hold values from -0.125 to 0.125
- w_value: bfloat16 [2048, 1024], P(None, 'tp'), may hold values from -0.125 to 0.125
- w_gate: bfloat16 [2048, 1024], P(None, 'tp'), may hold values from -0.125 to 0.125
- head_gain: bfloat16 [1024], P('tp'), may hold values from 0.099609375 to 1.8984375
- w_output: bfloat16 [1024, 2048], P('tp'), may hold values from -0.1875 to 0.1875
- state: float32 [1024, 8, 128, 128], P('ep', 'tp'), may hold values from -0.6 to 0.6
- positions: int32 [1024], P('ep'), may hold values from 1024 to 8191
- ffn_gain: bfloat16 [2048], replicated, may hold values from 0.099609375 to 1.8984375
- w_mix: bfloat16 [2048], replicated, may hold values from -0.125 to 0.125
- dense_gate: bfloat16 [2048, 5632], P('tp', 'ep'), may hold values from -0.125 to 0.125
- dense_up: bfloat16 [2048, 5632], P('tp', 'ep'), may hold values from -0.125 to 0.125
- dense_down: bfloat16 [5632, 2048], P('ep', 'tp'), may hold values from -0.15625 to 0.15625
- routes: int32 [1024, 2], P('ep'), may hold values from 0 to 31, all different within a row; in each aligned block of 32 rows (0 to 31, 32 to 63, ...) at most 4 rows name the same one
- route_weight: bfloat16 [1024, 2], P('ep'), may hold values from 0.19921875 to 1
- expert_gate: bfloat16 [32, 2048, 4096], P('ep', None, 'tp'), may hold values from -0.125 to 0.125
- expert_up: bfloat16 [32, 2048, 4096], P('ep', None, 'tp'), may hold values from -0.125 to 0.125
- expert_down: bfloat16 [32, 4096, 2048], P('ep', 'tp'), may hold values from -0.09375 to 0.09375
Outputs:
- final: bfloat16 [1024, 2048], P('ep', 'tp')
- new_state: float32 [1024, 8, 128, 128], P('ep', 'tp')
Inputs may be any that keep to these rules, and one draw needn't show every extreme that they name: `routes`: each row names 2 different experts; in the rows of one index of ep no expert is named by more than 4 rows, a bound that some block reaches; every expert is named by some row.
All inputs are finite; a program needn't handle non-finite values.
Results may differ from a plain program's by a relative error of at most 0.018.
Values may be sent and summed in bfloat16 or wider, within the bound.
No kernel may reach another device: no remote copies, remote signals or barrier semaphores. Data moves between devices by JAX's collectives and lax.ppermute only.
A program may use at most 64 MiB of HBM per device.

v0:
```python
import functools

import jax
import jax.numpy as jnp
from jax import lax
from jax.experimental import pallas as pl
from jax.experimental.pallas import tpu as pltpu
from jax.sharding import Mesh, PartitionSpec as P


EPSILON = 1e-06
THETA = 10000.0
EP = ("z", "x")
TP = ("y", "c")
BF = jnp.bfloat16
F32 = jnp.float32
VMEM = pl.BlockSpec(memory_space=pltpu.VMEM)
HBM = pl.BlockSpec(memory_space=pltpu.HBM)


def exchange(value, axis):
    return lax.all_to_all(value, axis, split_axis=0, concat_axis=0, tiled=True)


def swap_cores(value):
    return lax.ppermute(value, "c", [(0, 1), (1, 0)])


def dot(a, b):
    return jnp.dot(a, b, preferred_element_type=F32)


def dot_nt(a, b):
    return lax.dot_general(a, b, (((1,), (1,)), ((), ())), preferred_element_type=F32)


def dot_tn(a, b):
    return lax.dot_general(a, b, (((0,), (0,)), ((), ())), preferred_element_type=F32)


def silu(x):
    return x * jax.nn.sigmoid(x)


def iota(shape, dim):
    return lax.broadcasted_iota(jnp.int32, shape, dim)


def call(body, out_shape, in_specs, scratch=(), limit=16):
    many = isinstance(out_shape, (list, tuple))
    return pl.pallas_call(
        body, out_shape=out_shape, in_specs=in_specs,
        out_specs=[VMEM] * len(out_shape) if many else VMEM,
        scratch_shapes=list(scratch),
        compiler_params=pltpu.CompilerParams(vmem_limit_bytes=limit * 1024 * 1024),
    )


def place_of():
    core = lax.axis_index("c")
    return core, lax.axis_index("y") * lax.axis_size("c") + core


def head_body(
    inverse, resid, gain, places, head_gain, wq, wk, wv, wg, wo, state,
    partial, key_out, value_out,
    r_mem, gain_mem, p_mem, hg_mem, q_mem, k_mem, v_mem, g_mem, o_mem, state_mem, carried_mem, sems,
):
    pairs = [
        (resid, r_mem), (gain, gain_mem), (places, p_mem), (head_gain, hg_mem),
        (wq, q_mem), (wk, k_mem), (state, state_mem), (wv, v_mem), (wg, g_mem), (wo, o_mem),
    ]
    moves = [pltpu.make_async_copy(src, dst, sems.at[i]) for i, (src, dst) in enumerate(pairs)]
    for move in moves:
        move.start()
    seqs, width = r_mem.shape
    size = q_mem.shape[1]
    _, tp = place_of()
    for move in moves[:4]:
        move.wait()
    x = r_mem[...].astype(F32)
    square = jnp.mean(x * x, axis=-1, keepdims=True)
    x = x * lax.rsqrt(square + EPSILON)
    gains = gain_mem[...].astype(F32)
    lanes = gains.shape[1]
    normed = jnp.concatenate(
        [
            (x[:, b * lanes : (b + 1) * lanes] * gains[b : b + 1, :]).astype(BF)
            for b in range(width // lanes)
        ],
        axis=1,
    )
    row = jnp.broadcast_to(p_mem[...].astype(F32), (seqs, seqs))
    eye = iota((seqs, seqs), 0) == iota((seqs, seqs), 1)
    column = jnp.sum(jnp.where(eye, row, 0.0), axis=1, keepdims=True)
    angles = column * inverse[...]
    cosine = jnp.cos(angles)
    sine = jnp.where(iota((seqs, size), 1) < size // 2, -1.0, 1.0) * jnp.sin(angles)

    def rotate(value):
        return value * cosine + pltpu.roll(value, size // 2, 1) * sine

    def project(move, mem):
        move.wait()
        return dot(normed, mem[...]).astype(BF).astype(F32)

    query = rotate(project(moves[4], q_mem))
    key = rotate(project(moves[5], k_mem)) * size ** (-0.5)
    key_out[...] = key
    turned = query.T
    moves[6].wait()
    for s in range(seqs):
        carried_mem[s : s + 1, :] = jnp.sum(
            state_mem[s] * turned[:, s : s + 1], axis=0, keepdims=True
        )
    value = project(moves[7], v_mem)
    value_out[...] = value
    head = jnp.full((seqs, size), tp, jnp.int32).astype(F32)
    decay = 1.0 - jnp.exp2(-1.0 - 1.5 * head)
    mixture = jnp.sum(query * key, axis=-1, keepdims=True) * value + decay * carried_mem[...]
    centre = jnp.mean(mixture, axis=-1, keepdims=True)
    moved = mixture - centre
    spread = jnp.mean(moved * moved, axis=-1, keepdims=True)
    normed_head = moved * lax.rsqrt(spread + EPSILON) * hg_mem[...].astype(F32)
    retained = (silu(project(moves[8], g_mem)) * normed_head).astype(BF)
    moves[9].wait()
    cols = partial.shape[2]
    for i in range(partial.shape[0]):
        partial[i] = dot(retained, o_mem[:, i * cols : (i + 1) * cols]).astype(BF)


def middle_body(arrived, resid, routes, weights, outgoing, middle_out, weighing):
    _, tp = place_of()
    groups, seqs, cols = arrived.shape
    n_ep, rows, lanes = outgoing.shape
    pieces = cols // lanes
    n_x = lax.axis_size("x")
    share = seqs // n_x
    per = rows - pieces * share
    slots = per // pieces

    def mask(value):
        return value.astype(F32).astype(BF)

    expert = iota((n_ep, seqs), 0)
    named = [expert == routes[j : j + 1, :] for j in range(routes.shape[0])]
    weight_of, hit = 0.0, 0.0
    for j, here in enumerate(named):
        hit = hit + here.astype(F32)
        weight_of = weight_of + jnp.where(here, weights[j : j + 1, :].astype(F32), 0.0)
    earlier = mask(iota((seqs, seqs), 0) < iota((seqs, seqs), 1))
    rank = jnp.where(hit > 0.5, dot(hit.astype(BF), earlier), 2.0 * seqs).astype(BF)
    shape = (n_ep * per, seqs)
    to = iota(shape, 0)
    repeat = mask(iota((n_ep * per, n_ep), 0) // per == iota((n_ep * per, n_ep), 1))
    taken = dot(repeat, rank) == (to % slots).astype(F32)
    weight_of = dot(repeat, weight_of.astype(BF))
    picks = []
    for h in range(pieces):
        here = taken & (to // slots % pieces == h)
        picks.append(mask(here))
        weighing[h] = jnp.where(here, weight_of, 0.0).astype(BF)
    shape = (n_ep * share, seqs)
    to = iota(shape, 0)
    dense_pick = mask(iota(shape, 1) == to // share % n_x * share + to % share)

    total = resid[:, pl.ds(pl.multiple_of(tp * cols, cols), cols)].astype(F32)
    for i in range(groups):
        total = total + arrived[i].astype(F32)
    middle_out[...] = total
    cut = total.astype(BF)
    chosen = 0.0
    for h in range(pieces):
        part = cut[:, h * lanes : (h + 1) * lanes]
        dense = dot(dense_pick, part).astype(BF)
        outgoing[:, h * share : (h + 1) * share, :] = dense.reshape(n_ep, share, lanes)
        chosen = chosen + dot(picks[h], part)
    outgoing[:, pieces * share :, :] = chosen.astype(BF).reshape(n_ep, per, lanes)


def dense_body(own, other, gains, mixers, *rest):
    out = rest[-1]
    n_x = lax.axis_size("x")
    n_blocks = len(rest) // 2
    weights, weights_other = rest[:n_blocks], rest[n_blocks : 2 * n_blocks]
    core, tp = place_of()
    sources, _, lanes = own.shape
    n_y = out.shape[0]
    hids, cols = weights[0].shape
    pieces = cols // lanes
    share = 32 // n_x
    slots = own.shape[1] // pieces - share
    n_slots = sources * slots
    top = hids + 16
    shape = (pieces * n_slots, pieces * n_slots)
    to, at = iota(shape, 0), iota(shape, 1)
    row = to % n_slots
    turn = at == row // slots * (pieces * slots) + to // n_slots * slots + row % slots
    turn = turn.astype(F32).astype(BF)

    def expert_rows(ref, which):
        rows = ref[:, pieces * share :, :].reshape(pieces * n_slots, lanes)
        rows = dot(turn, rows).astype(BF)
        start = pl.multiple_of(top + which * pieces * n_slots, 16)
        for i in range(n_y):
            out[i, pl.ds(start, pieces * n_slots), :] = rows

    expert_rows(own, core)
    expert_rows(other, 1 - core)

    def columns(ref, which):
        table = ref[...].astype(F32)
        picked = [
            jnp.sum(jnp.where(iota(table.shape, 0) == which * pieces + h, table, 0.0),
                    axis=0, keepdims=True)
            for h in range(pieces)
        ]
        return jnp.concatenate(picked, axis=1)

    def dense_rows(ref):
        return jnp.concatenate(
            [
                ref[:, h * share : (h + 1) * share, :].reshape(sources * share, lanes).astype(F32)
                for h in range(pieces)
            ],
            axis=1,
        )

    mine, theirs = dense_rows(own), dense_rows(other)
    x = (mine * columns(gains, tp)).astype(BF)
    x_other = (theirs * columns(gains, tp ^ 1)).astype(BF)
    ones = jnp.ones((16, cols), BF)
    squares = dot_nt(ones, (mine * mine).astype(BF)) + dot_nt(ones, (theirs * theirs).astype(BF))

    def mixer(which):
        return jnp.broadcast_to(columns(mixers, which), (16, cols)).astype(BF)

    mixes = dot_nt(mixer(tp), x) + dot_nt(mixer(tp ^ 1), x_other)
    low = jnp.where(iota(mixes.shape, 0) == 0, mixes, squares).astype(BF)
    halves = n_y // n_blocks
    for k in range(n_blocks):
        sums = (dot_nt(weights[k][...], x) + dot_nt(weights_other[k][...], x_other)).astype(BF)
        for t in range(halves):
            part = slice(t * lanes, (t + 1) * lanes)
            out[k * halves + t, 0:hids, :] = sums[:, part]
            out[k * halves + t, hids:top, :] = low[:, part]


def expert_body(
    got, gain, gate, up, hidden_out, expert_out, x_mem
):
    n_y, _, lanes = got.shape
    hid = hidden_out.shape[0]
    n_slots, width = x_mem.shape
    top = 2 * hid + 16
    per_y = width // n_y // lanes
    square = jnp.zeros((n_slots, 1), F32)
    for b in range(width // lanes):
        start = top + b % per_y * n_slots
        piece = got[b // per_y, start : start + n_slots, :].astype(F32)
        square = square + jnp.sum(piece * piece, axis=1, keepdims=True)
    scale = lax.rsqrt(square / width + EPSILON)
    gains = gain[...].astype(F32)
    for b in range(width // lanes):
        start = top + b % per_y * n_slots
        piece = got[b // per_y, start : start + n_slots, :].astype(F32)
        part = slice(b * lanes, (b + 1) * lanes)
        x_mem[:, part] = (piece * scale * gains[b : b + 1, :]).astype(BF)

    sums = got[0, 0:top, :].astype(F32)
    for i in range(1, n_y):
        sums = sums + got[i, 0:top, :].astype(F32)
    factor = lax.rsqrt(sums[2 * hid + 1 : 2 * hid + 2] / width + EPSILON)
    mixing = jax.nn.sigmoid(sums[2 * hid : 2 * hid + 1] * factor)
    dense = silu(sums[:hid] * factor) * (sums[hid : 2 * hid] * factor) * mixing
    hidden_out[...] = dense.astype(BF)

    gates = dot(x_mem[...], gate[0])
    ups = dot(x_mem[...], up[0])
    expert_out[...] = (silu(gates) * ups).astype(BF)


def down_body(other, hidden, down, out):
    core, _ = place_of()
    which = core ^ other
    n_y, _, cols = out.shape
    for i in range(n_y):
        start = pl.multiple_of(which * cols + i * 2 * cols, cols)
        out[i] = dot(hidden[...], down[0, :, pl.ds(start, cols)]).astype(BF)


def pair_body(keep, got, hidden, hidden_other, out):
    core, _ = place_of()
    n_y, n_slots, cols = keep.shape
    lanes = out.shape[2]
    hid = hidden.shape[0]
    at = cols // lanes * n_slots
    for i in range(n_y):
        total = (keep[i].astype(F32) + got[i].astype(F32)).astype(BF)
        for h in range(cols // lanes):
            out[i, h * n_slots : (h + 1) * n_slots, :] = total[:, h * lanes : (h + 1) * lanes]
        out[i, pl.ds(pl.multiple_of(at + core * hid, 16), hid), :] = hidden[...]
        out[i, pl.ds(pl.multiple_of(at + (1 - core) * hid, 16), hid), :] = hidden_other[...]


def back_body(got, *rest):
    downs, out = rest[:-1], rest[-1]
    n_x = len(downs)
    n_y, _, lanes = got.shape
    hid, cols = downs[0].shape
    sources = out.shape[0]
    pieces = cols // lanes
    at = got.shape[1] - 2 * hid
    slots = at // pieces // sources
    share = out.shape[1] // pieces - slots
    result = got[0, 0:at, :].astype(F32)
    for i in range(1, n_y):
        result = result + got[i, 0:at, :].astype(F32)
    to = iota((at, at), 0)
    source, piece, slot = to // (pieces * slots), to // slots % pieces, to % slots
    turn = (iota((at, at), 1) == piece * (at // pieces) + source * slots + slot).astype(F32)
    result = dot(turn.astype(BF), result.astype(BF)).astype(BF)
    out[:, pieces * share :, :] = result.reshape(sources, pieces * slots, lanes)
    halves = sources * share // lanes
    blocks = n_y // halves
    half = sources // halves
    for t in range(halves):
        total = 0.0
        for k in range(n_x):
            c, i = k // blocks, k % blocks * halves + t
            total = total + dot_tn(got[i, at + c * hid : at + (c + 1) * hid, :], downs[k][...])
        total = total.astype(BF)
        for h in range(pieces):
            out[t * half : (t + 1) * half, h * share : (h + 1) * share, :] = total[
                :, h * lanes : (h + 1) * lanes
            ].reshape(half, share, lanes)


def final_body(back, weighing, middle, out):
    sources, _, lanes = back.shape
    seqs, cols = middle.shape
    pieces = cols // lanes
    n_x = lax.axis_size("x")
    share = seqs // n_x
    experts = back[:, pieces * share :, :].reshape(-1, lanes)
    for h in range(pieces):
        part = slice(h * lanes, (h + 1) * lanes)
        rows = slice(h * share, (h + 1) * share)
        dense = []
        for x in range(n_x):
            total = back[x, rows, :].astype(F32)
            for z in range(1, sources // n_x):
                total = total + back[z * n_x + x, rows, :].astype(F32)
            dense.append(total)
        total = jnp.concatenate(dense, axis=0) + dot_tn(weighing[h], experts)
        out[:, part] = (middle[:, part] + total).astype(BF)


def one_device(
    resid, norm_gain, w_query, w_key, w_value, w_gate, head_gain, w_output, state, positions,
    ffn_gain, w_mix, dense_gate, dense_up, dense_down, routes, route_weight,
    expert_gate, expert_up, expert_down,
):
    sds = jax.ShapeDtypeStruct
    seqs, width = resid.shape
    n_y, n_c, n_x = lax.axis_size("y"), lax.axis_size("c"), lax.axis_size("x")
    n_tp = n_y * n_c
    n_ep = lax.axis_size("z") * n_x
    cols = width // n_tp
    tp = lax.axis_index("y") * n_c + lax.axis_index("c")
    slots = max(2, 2 * seqs * routes.shape[1] // n_ep)
    n_slots = n_ep * slots
    hid = dense_gate.shape[1]
    size = state.shape[2]
    lanes = 128
    pieces = cols // lanes
    share = seqs // n_x

    steps = jnp.arange(size, dtype=jnp.int32) % (size // 2)
    inverse = (THETA ** (-steps.astype(F32) / (size // 2)))[None, :]
    partial, key, value = call(
        head_body,
        [sds((n_tp, seqs, cols), BF), sds((seqs, size), F32), sds((seqs, size), F32)],
        [VMEM] + [HBM] * 10,
        [pltpu.VMEM((seqs, width), BF), pltpu.VMEM((width // lanes, lanes), BF),
         pltpu.VMEM((1, seqs), jnp.int32), pltpu.VMEM((1, size), BF)]
        + [pltpu.VMEM((width, size), BF)] * 4
        + [pltpu.VMEM((size, width), BF), pltpu.VMEM((seqs, size, size), F32),
           pltpu.VMEM((seqs, size), F32), pltpu.SemaphoreType.DMA((10,))],
    )(inverse, *(pltpu.with_memory_space_constraint(w, pltpu.HBM) for w in (
        resid, norm_gain.reshape(width // lanes, lanes), positions[None], head_gain[None],
        w_query, w_key, w_value, w_gate, w_output, state.reshape(seqs, size, size))))
    decay = 1.0 - jnp.exp2(-1.0 - 1.5 * tp.astype(F32))
    new_state = decay * state + (key[:, :, None] * value[:, None, :])[:, None]
    arrived = exchange(partial, TP)

    blocks = n_x // n_c
    both = jnp.concatenate([dense_gate.T, dense_up.T], axis=0)

    def piece(block, other):
        pairs = []
        for x in range(n_x):
            for c in range(n_c):
                source = (x + blocks * c + block) % n_x * n_c + (c ^ other)
                pairs.append((source, x * n_c + c))
        return lax.ppermute(both, ("x", "c"), pairs)

    weights = [piece(k, 0) for k in range(blocks)]
    weights_other = [piece(k, 1) for k in range(blocks)]
    downs = [dense_down] + [
        lax.ppermute(dense_down, "x", [((i + k) % n_x, i) for i in range(n_x)])
        for k in range(1, n_x)
    ]

    outgoing, middle, weighing = call(
        middle_body,
        [sds((n_ep, pieces * (share + slots), lanes), BF), sds((seqs, cols), F32),
         sds((pieces, pieces * n_slots, seqs), BF)],
        [VMEM] * 4,
    )(arrived, resid, routes.T, route_weight.T)
    rows = exchange(outgoing, EP)

    def table(value):
        return value.reshape(width // lanes, lanes)

    rows_other = swap_cores(rows)
    sent = call(
        dense_body, sds((n_y, 2 * hid + 16 + n_c * pieces * n_slots, lanes), BF),
        [VMEM] * (4 + 2 * blocks),
    )(rows, rows_other, table(ffn_gain), table(w_mix), *weights, *weights_other)
    got = exchange(sent, "y")

    hidden, expert_hidden = call(
        expert_body,
        [sds((hid, lanes), BF), sds((n_slots, expert_gate.shape[2]), BF)],
        [VMEM] * 4,
        [pltpu.VMEM((n_slots, width), BF)],
    )(got, table(ffn_gain), expert_gate, expert_up)

    def down_half(other):
        return call(
            functools.partial(down_body, other),
            sds((n_y, n_slots, cols), BF), [VMEM] * 2,
        )(expert_hidden, expert_down)

    send = down_half(1)
    half = swap_cores(send)
    keep = down_half(0)
    sent = call(
        pair_body, sds((n_y, pieces * n_slots + n_c * hid, lanes), BF), [VMEM] * 4,
    )(keep, half, hidden, swap_cores(hidden))
    got = exchange(sent, "y")

    back = call(
        back_body, sds((n_ep, pieces * (share + slots), lanes), BF),
        [VMEM] * (1 + n_x),
    )(got, *downs)
    back = exchange(back, EP)

    final = call(final_body, sds((seqs, cols), BF), [VMEM] * 3)(back, weighing, middle)
    return (final, new_state)


def solution(mesh):
    inner = Mesh(mesh.devices.reshape(8, 4, 4, 2), ("z", "x", "y", "c"))
    in_specs = (
        P(EP, None), P(), P(None, TP), P(None, TP), P(None, TP), P(None, TP), P(TP), P(TP, None),
        P(EP, TP, None, None), P(EP), P(), P(), P(TP, EP), P(TP, EP), P(EP, TP),
        P(EP, None), P(EP, None), P(EP, None, TP), P(EP, None, TP), P(EP, TP, None),
    )
    out_specs = (P(EP, TP), P(EP, TP, None, None))
    return jax.shard_map(
        one_device, mesh=inner, in_specs=in_specs, out_specs=out_specs, check_vma=False
    )
```

profile of v0, /device:TPU:24, one launch (start us, length us, event | category | flops | bytes accessed | tf_op | source)
XLA Modules:
  0.0 103.2 jit_solution(3580358311680060177)
XLA Ops:
  0.6 0.0 copy-start.3
  0.7 0.0 copy-start.7
  0.7 0.0 copy-start.8
  0.7 0.0 copy-start.10
  0.7 0.0 copy-start.11
  0.7 0.0 copy-start.5
  0.7 0.0 copy-start.6
  0.7 3.7 %shard_map.203 = (bf16[8,32,256]{2,1,0:T(8,128)(2,1)S(1)}, f32[32,128]{1,0:T(8,128)S(1)}, f32[32,128]{1,0:T(8,128)S(1)}) custom-call(f32[1,128]{1,0:T(1,128)S(1)} %fusion.3.inverse, bf16[32,2048]{1,0:T(8,128)(2,1)} %resid.3, bf16[16,128]{1,0:T(8,128)(2,1)} %bitcast.18, s32[1,32]{1,0:T(1,128)} %bitcast.19, bf16[1,128]{1,0:T(2,128)(2,1)} %bitcast.20, ...), custom_call_target="tpu_custom_call" | custom-call | tf_op jit(solution)/shard_map/pallas_call | solution.py:381
  4.4 8.5 %all_to_all.25.arrived = bf16[8,32,256]{2,1,0:T(8,128)(2,1)S(1)} all-to-all(bf16[8,32,256]{2,1,0:T(8,128)(2,1)S(1)} %get-tuple-element.10), channel_id=1, replica_groups=mesh['z'=8,'x'=4,'y'=4,'c'=2] {'y','c'}, dimensions={0} | all-to-all | bytes 262144 | tf_op jit(solution)/shard_map/all_to_all | solution.py:22
  12.9 0.0 copy-done.3
  12.9 0.0 copy-done.7
  13.0 0.0 copy-done.8
  13.0 0.5 shard_map.204
  13.5 0.0 copy-start.2
  13.5 22.8 %all_to_all.26.own = bf16[32,24,128]{2,1,0:T(8,128)(2,1)S(1)} all-to-all(bf16[32,24,128]{2,1,0:T(8,128)(2,1)S(1)} %get-tuple-element.11), channel_id=1, replica_groups=mesh['z'=8,'x'=4,'y'=4,'c'=2] {'z','x'}, dimensions={0} | all-to-all | bytes 393216 | tf_op jit(solution)/shard_map/all_to_all | solution.py:22
  36.2 0.0 copy-start.1
  36.2 0.0 collective-permute-start
  36.2 0.0 copy-done.10
  36.2 0.0 copy-done.11
  36.3 0.8 collective-permute-start.1
  37.1 1.3 %collective-permute-start.2 = (bf16[352,256]{1,0:T(8,128)(2,1)S(1)}, bf16[352,256]{1,0:T(8,128)(2,1)S(1)}, u32[]{:S(2)}, u32[]{:S(2)}) collective-permute-start(bf16[352,256]{1,0:T(8,128)(2,1)S(1)} %pad_maximum_fusion), channel_id=1, source_target_pairs={{8,0},{25,1},{16,8},{1,9},{24,16},{9,17},{0,24},{17,25},{10,2},{27... | collective-permute-start | bytes 540680 | tf_op jit(solution)/shard_map/ppermute | solution.py:406
  38.3 3.5 %collective-permute-start.3 = (bf16[352,256]{1,0:T(8,128)(2,1)S(1)}, bf16[352,256]{1,0:T(8,128)(2,1)S(1)}, u32[]{:S(2)}, u32[]{:S(2)}) collective-permute-start(bf16[352,256]{1,0:T(8,128)(2,1)S(1)} %pad_maximum_fusion), channel_id=1, source_target_pairs={{1,0},{16,1},{9,8},{24,9},{17,16},{0,17},{25,24},{8,25},{3,2},{18,... | collective-permute-start | bytes 540680 | tf_op jit(solution)/shard_map/ppermute | solution.py:406
  41.8 0.0 collective-permute-start.4
  41.8 0.0 collective-permute-done.1.rest_0_
  41.8 2.2 %collective-permute-done.2.rest_1_ = bf16[352,256]{1,0:T(8,128)(2,1)S(1)} collective-permute-done((bf16[352,256]{1,0:T(8,128)(2,1)S(1)}, bf16[352,256]{1,0:T(8,128)(2,1)S(1)}, u32[]{:S(2)}, u32[]{:S(2)}) %collective-permute-start.2) | collective-permute-done | bytes 180256 | tf_op jit(solution)/shard_map/ppermute | solution.py:406
  44.0 1.9 %collective-permute-done.3.rest_2_ = bf16[352,256]{1,0:T(8,128)(2,1)S(1)} collective-permute-done((bf16[352,256]{1,0:T(8,128)(2,1)S(1)}, bf16[352,256]{1,0:T(8,128)(2,1)S(1)}, u32[]{:S(2)}, u32[]{:S(2)}) %collective-permute-start.3) | collective-permute-done | bytes 180256 | tf_op jit(solution)/shard_map/ppermute | solution.py:406
  46.0 2.7 %collective-permute-done.4.rest_3_ = bf16[352,256]{1,0:T(8,128)(2,1)S(1)} collective-permute-done((bf16[352,256]{1,0:T(8,128)(2,1)S(1)}, bf16[352,256]{1,0:T(8,128)(2,1)S(1)}, u32[]{:S(2)}, u32[]{:S(2)}) %collective-permute-start.4) | collective-permute-done | bytes 180256 | tf_op jit(solution)/shard_map/ppermute | solution.py:406
  48.7 0.0 collective-permute-done.other
  48.7 0.0 copy-done.5
  48.7 0.0 copy-done.6
  48.7 0.6 shard_map.205
  49.3 16.7 %all_to_all.27.got = bf16[4,880,128]{2,1,0:T(8,128)(2,1)S(1)} all-to-all(bf16[4,880,128]{2,1,0:T(8,128)(2,1)S(1)} %shard_map.205), channel_id=1, replica_groups=mesh['z'=8,'x'=4,'y'=4,'c'=2] {'y'}, dimensions={0} | all-to-all | bytes 1802240 | tf_op jit(solution)/shard_map/all_to_all | solution.py:22
  66.0 0.0 copy-done.2
  66.0 0.0 copy-done.1
  66.0 0.0 copy-start
  66.0 1.1 %shard_map.206 = (bf16[176,128]{1,0:T(8,128)(2,1)S(1)}, bf16[128,512]{1,0:T(8,128)(2,1)S(1)}) custom-call(bf16[4,880,128]{2,1,0:T(8,128)(2,1)S(1)} %all_to_all.27.got, bf16[16,128]{1,0:T(8,128)(2,1)S(1)} %bitcast.11, bf16[1,2048,512]{2,1,0:T(8,128)(2,1)S(1)} %copy-done.1, bf16[1,2048,512]{2,1,0:T(8,128)(2,1)S(1)} %copy-done.2), custom_call_target="tpu_custom_call" | custom-call | tf_op jit(solution)/shard_map/pallas_call | solution.py:433
  67.0 0.5 copy-done
  67.6 0.3 shard_map.208
  67.9 0.6 collective-permute-start.5
  68.5 0.0 copy-start.4
  68.5 0.1 collective-permute-start.6
  68.6 0.3 shard_map.207.keep
  68.9 0.0 copy-start.9
  68.9 0.8 collective-permute-done.6.hidden_other
  69.7 0.0 collective-permute-done.5.got
  69.7 0.9 shard_map.209
  70.6 5.5 %all-to-all-start.3 = ((bf16[4,608,128]{2,1,0:T(8,128)(2,1)}), bf16[4,608,128]{2,1,0:T(8,128)(2,1)S(1)}, u32[]{:S(2)}, u32[]{:S(2)}) async-start(bf16[4,608,128]{2,1,0:T(8,128)(2,1)} %shard_map.209), calls=%async_computation.3 | async-start | bytes 1245184 | tf_op jit(solution)/shard_map/all_to_all | solution.py:22
  76.1 0.0 copy-done.4
  76.1 2.2 %collective-permute-start.7 = (bf16[176,256]{1,0:T(8,128)(2,1)S(1)}, bf16[176,256]{1,0:T(8,128)(2,1)S(1)}, u32[]{:S(2)}, u32[]{:S(2)}) collective-permute-start(bf16[176,256]{1,0:T(8,128)(2,1)S(1)} %copy-done.4), channel_id=1, source_target_pairs={{8,0},{16,8},{24,16},{0,24},{9,1},{17,9},{25,17},{1,25},{10,2},{18... | collective-permute-start | bytes 270344 | tf_op jit(solution)/shard_map/ppermute | solution.py:411
  78.4 1.0 %collective-permute-start.8 = (bf16[176,256]{1,0:T(8,128)(2,1)S(1)}, bf16[176,256]{1,0:T(8,128)(2,1)S(1)}, u32[]{:S(2)}, u32[]{:S(2)}) collective-permute-start(bf16[176,256]{1,0:T(8,128)(2,1)S(1)} %copy-done.4), channel_id=1, source_target_pairs={{16,0},{24,8},{0,16},{8,24},{17,1},{25,9},{1,17},{9,25},{18,2},{26... | collective-permute-start | bytes 270344 | tf_op jit(solution)/shard_map/ppermute | solution.py:411
  79.4 0.0 collective-permute-start.9
  79.4 2.8 %collective-permute-done.7.rest_1_ = bf16[176,256]{1,0:T(8,128)(2,1)S(1)} collective-permute-done((bf16[176,256]{1,0:T(8,128)(2,1)S(1)}, bf16[176,256]{1,0:T(8,128)(2,1)S(1)}, u32[]{:S(2)}, u32[]{:S(2)}) %collective-permute-start.7) | collective-permute-done | bytes 90144 | tf_op jit(solution)/shard_map/ppermute | solution.py:411
  82.2 2.7 %collective-permute-done.8.rest_2_ = bf16[176,256]{1,0:T(8,128)(2,1)S(1)} collective-permute-done((bf16[176,256]{1,0:T(8,128)(2,1)S(1)}, bf16[176,256]{1,0:T(8,128)(2,1)S(1)}, u32[]{:S(2)}, u32[]{:S(2)}) %collective-permute-start.8) | collective-permute-done | bytes 90144 | tf_op jit(solution)/shard_map/ppermute | solution.py:411
  84.9 1.0 collective-permute-done.9.rest_3_
  85.9 0.0 all-to-all-done.3.got
  85.9 1.1 %shard_map.210 = bf16[32,24,128]{2,1,0:T(8,128)(2,1)} custom-call(bf16[4,608,128]{2,1,0:T(8,128)(2,1)S(1)} %all-to-all-done.3.got, bf16[176,256]{1,0:T(8,128)(2,1)S(1)} %copy-done.4, bf16[176,256]{1,0:T(8,128)(2,1)S(1)} %collective-permute-done.7.rest_1_, bf16[176,256]{1,0:T(8,128)(2,1)S(1)} %collective-permute-done.8.rest_2_, ...), custom_call_target="tpu_custom_call" | custom-call | tf_op jit(solution)/shard_map/pallas_call | solution.py:454
  87.0 3.9 %all-to-all-start.4 = ((bf16[32,24,128]{2,1,0:T(8,128)(2,1)}), bf16[32,24,128]{2,1,0:T(8,128)(2,1)S(1)}, u32[]{:S(2)}, u32[]{:S(2)}) async-start(bf16[32,24,128]{2,1,0:T(8,128)(2,1)} %shard_map.210), calls=%async_computation.4 | async-start | bytes 393216 | tf_op jit(solution)/shard_map/all_to_all | solution.py:22
  90.9 0.0 copy-done.9
  90.9 1.7 %multiply_add_fusion = f32[32,1,128,128]{3,2,1,0:T(8,128)} fusion(f32[32,1,128,128]{3,2,1,0:T(8,128)S(1)} %copy-done.9, f32[32,128]{1,0:T(8,128)S(1)} %get-tuple-element.17, f32[32,128]{1,0:T(8,128)S(1)} %get-tuple-element.16, f32[]{:T(128)S(6)} %sub.7), kind=kLoop, calls=%fused_computation | loop fusion | flops 1572864 | bytes 4227076 | tf_op jit(solution)/shard_map/add | solution.py:394
  92.6 9.8 %all-to-all-done.4.back = bf16[32,24,128]{2,1,0:T(8,128)(2,1)S(1)} async-done(((bf16[32,24,128]{2,1,0:T(8,128)(2,1)}), bf16[32,24,128]{2,1,0:T(8,128)(2,1)S(1)}, u32[]{:S(2)}, u32[]{:S(2)}) %all-to-all-start.4) | async-done | bytes 196640 | tf_op jit(solution)/shard_map/all_to_all | solution.py:22
  102.4 0.8 shard_map.211
  (2 shorter events, 0.0 us)
Async XLA Ops:
  0.6 12.3 %copy-start.3 = (bf16[32,2048]{1,0:T(8,128)(2,1)S(1)}, bf16[32,2048]{1,0:T(8,128)(2,1)}, u32[]{:S(2)}) copy-start(bf16[32,2048]{1,0:T(8,128)(2,1)} %resid.3) | copy-start | bytes 393220
  0.7 12.3 %copy-start.7 = (s32[32,2]{0,1:T(2,128)S(1)}, s32[32,2]{0,1:T(2,128)}, u32[]{:S(2)}) copy-start(s32[32,2]{0,1:T(2,128)} %param.35) | copy-start | bytes 772
  0.7 12.3 %copy-start.8 = (bf16[32,2]{0,1:T(2,128)(2,1)S(1)}, bf16[32,2]{0,1:T(2,128)(2,1)}, u32[]{:S(2)}) copy-start(bf16[32,2]{0,1:T(2,128)(2,1)} %param.36) | copy-start | bytes 388
  0.7 35.6 %copy-start.10 = (bf16[256,176]{0,1:T(8,128)(2,1)S(1)}, bf16[256,176]{0,1:T(8,128)(2,1)}, u32[]{:S(2)}) copy-start(bf16[256,176]{0,1:T(8,128)(2,1)} %param.33) | copy-start | bytes 270340
  0.7 35.6 %copy-start.11 = (bf16[256,176]{0,1:T(8,128)(2,1)S(1)}, bf16[256,176]{0,1:T(8,128)(2,1)}, u32[]{:S(2)}) copy-start(bf16[256,176]{0,1:T(8,128)(2,1)} %param.32) | copy-start | bytes 270340
  0.7 48.0 %copy-start.5 = (bf16[2048]{0:T(1024)(128)(2,1)S(1)}, bf16[2048]{0:T(1024)(128)(2,1)}, u32[]{:S(2)}) copy-start(bf16[2048]{0:T(1024)(128)(2,1)} %param.30) | copy-start | bytes 12292
  0.7 48.0 %copy-start.6 = (bf16[2048]{0:T(1024)(128)(2,1)S(1)}, bf16[2048]{0:T(1024)(128)(2,1)}, u32[]{:S(2)}) copy-start(bf16[2048]{0:T(1024)(128)(2,1)} %param.31) | copy-start | bytes 12292
  13.5 52.5 %copy-start.2 = (bf16[1,2048,512]{2,1,0:T(8,128)(2,1)S(1)}, bf16[1,2048,512]{2,1,0:T(8,128)(2,1)}, u32[]{:S(2)}) copy-start(bf16[1,2048,512]{2,1,0:T(8,128)(2,1)} %up.1) | copy-start | bytes 6291460
  36.2 29.7 %copy-start.1 = (bf16[1,2048,512]{2,1,0:T(8,128)(2,1)S(1)}, bf16[1,2048,512]{2,1,0:T(8,128)(2,1)}, u32[]{:S(2)}) copy-start(bf16[1,2048,512]{2,1,0:T(8,128)(2,1)} %gate.1) | copy-start | bytes 6291460
  36.2 12.4 %collective-permute-start = (bf16[32,24,128]{2,1,0:T(8,128)(2,1)S(1)}, bf16[32,24,128]{2,1,0:T(8,128)(2,1)S(1)}, u32[]{:S(2)}, u32[]{:S(2)}) collective-permute-start(bf16[32,24,128]{2,1,0:T(8,128)(2,1)S(1)} %all_to_all.26.own), channel_id=1, source_target_pairs={{0,1},{1,0},{2,3},{3,2},{4,5},{5,4},{6,7},{7,6},{8,9},{9,8},{10,11... | collective-permute-start | bytes 589832 | tf_op jit(solution)/shard_map/ppermute | solution.py:26
  36.3 5.6 %collective-permute-start.1 = (bf16[352,256]{1,0:T(8,128)(2,1)S(1)}, bf16[352,256]{1,0:T(8,128)(2,1)S(1)}, u32[]{:S(2)}, u32[]{:S(2)}) collective-permute-start(bf16[352,256]{1,0:T(8,128)(2,1)S(1)} %pad_maximum_fusion), channel_id=1, source_target_pairs={{0,0},{17,1},{8,8},{25,9},{16,16},{1,17},{24,24},{9,25},{2,2},{19,... | collective-permute-start | bytes 540680 | tf_op jit(solution)/shard_map/ppermute | solution.py:406
  37.1 7.0 %collective-permute-start.2 = (bf16[352,256]{1,0:T(8,128)(2,1)S(1)}, bf16[352,256]{1,0:T(8,128)(2,1)S(1)}, u32[]{:S(2)}, u32[]{:S(2)}) collective-permute-start(bf16[352,256]{1,0:T(8,128)(2,1)S(1)} %pad_maximum_fusion), channel_id=1, source_target_pairs={{8,0},{25,1},{16,8},{1,9},{24,16},{9,17},{0,24},{17,25},{10,2},{27... | collective-permute-start | bytes 540680 | tf_op jit(solution)/shard_map/ppermute | solution.py:406
  38.3 7.6 %collective-permute-start.3 = (bf16[352,256]{1,0:T(8,128)(2,1)S(1)}, bf16[352,256]{1,0:T(8,128)(2,1)S(1)}, u32[]{:S(2)}, u32[]{:S(2)}) collective-permute-start(bf16[352,256]{1,0:T(8,128)(2,1)S(1)} %pad_maximum_fusion), channel_id=1, source_target_pairs={{1,0},{16,1},{9,8},{24,9},{17,16},{0,17},{25,24},{8,25},{3,2},{18,... | collective-permute-start | bytes 540680 | tf_op jit(solution)/shard_map/ppermute | solution.py:406
  41.8 6.8 %collective-permute-start.4 = (bf16[352,256]{1,0:T(8,128)(2,1)S(1)}, bf16[352,256]{1,0:T(8,128)(2,1)S(1)}, u32[]{:S(2)}, u32[]{:S(2)}) collective-permute-start(bf16[352,256]{1,0:T(8,128)(2,1)S(1)} %pad_maximum_fusion), channel_id=1, source_target_pairs={{9,0},{24,1},{17,8},{0,9},{25,16},{8,17},{1,24},{16,25},{11,2},{26... | collective-permute-start | bytes 540680 | tf_op jit(solution)/shard_map/ppermute | solution.py:406
  66.0 1.6 %copy-start = (bf16[1,512,2048]{2,1,0:T(8,128)(2,1)S(1)}, bf16[1,512,2048]{2,1,0:T(8,128)(2,1)}, u32[]{:S(2)}) copy-start(bf16[1,512,2048]{2,1,0:T(8,128)(2,1)} %down.3) | copy-start | bytes 6291460
  67.9 1.8 %collective-permute-start.5 = (bf16[4,128,256]{2,1,0:T(8,128)(2,1)S(1)}, bf16[4,128,256]{2,1,0:T(8,128)(2,1)S(1)}, u32[]{:S(2)}, u32[]{:S(2)}) collective-permute-start(bf16[4,128,256]{2,1,0:T(8,128)(2,1)S(1)} %shard_map.208), channel_id=1, source_target_pairs={{0,1},{1,0},{2,3},{3,2},{4,5},{5,4},{6,7},{7,6},{8,9},{9,8},{10,11... | collective-permute-start | bytes 786440 | tf_op jit(solution)/shard_map/ppermute | solution.py:26
  68.5 7.7 %copy-start.4 = (bf16[176,256]{1,0:T(8,128)(2,1)S(1)}, bf16[176,256]{1,0:T(8,128)(2,1)}, u32[]{:S(2)}) copy-start(bf16[176,256]{1,0:T(8,128)(2,1)} %rest_0_.1) | copy-start | bytes 270340
  68.5 1.2 %collective-permute-start.6 = (bf16[176,128]{1,0:T(8,128)(2,1)S(1)}, bf16[176,128]{1,0:T(8,128)(2,1)S(1)}, u32[]{:S(2)}, u32[]{:S(2)}) collective-permute-start(bf16[176,128]{1,0:T(8,128)(2,1)S(1)} %get-tuple-element.13.hidden), channel_id=1, source_target_pairs={{0,1},{1,0},{2,3},{3,2},{4,5},{5,4},{6,7},{7,6},{8,9},{9,8},{10,11... | collective-permute-start | bytes 135176 | tf_op jit(solution)/shard_map/ppermute | solution.py:26
  68.9 22.0 %copy-start.9 = (f32[32,1,128,128]{3,2,1,0:T(8,128)S(1)}, f32[32,1,128,128]{3,2,1,0:T(8,128)}, u32[]{:S(2)}) copy-start(f32[32,1,128,128]{3,2,1,0:T(8,128)} %param.28) | copy-start | bytes 6291460
  70.6 15.3 %all-to-all-start.3 = ((bf16[4,608,128]{2,1,0:T(8,128)(2,1)}), bf16[4,608,128]{2,1,0:T(8,128)(2,1)S(1)}, u32[]{:S(2)}, u32[]{:S(2)}) async-start(bf16[4,608,128]{2,1,0:T(8,128)(2,1)} %shard_map.209), calls=%async_computation.3 | async-start | bytes 1245184 | tf_op jit(solution)/shard_map/all_to_all | solution.py:22
  76.1 6.1 %collective-permute-start.7 = (bf16[176,256]{1,0:T(8,128)(2,1)S(1)}, bf16[176,256]{1,0:T(8,128)(2,1)S(1)}, u32[]{:S(2)}, u32[]{:S(2)}) collective-permute-start(bf16[176,256]{1,0:T(8,128)(2,1)S(1)} %copy-done.4), channel_id=1, source_target_pairs={{8,0},{16,8},{24,16},{0,24},{9,1},{17,9},{25,17},{1,25},{10,2},{18... | collective-permute-start | bytes 270344 | tf_op jit(solution)/shard_map/ppermute | solution.py:411
  78.4 6.6 %collective-permute-start.8 = (bf16[176,256]{1,0:T(8,128)(2,1)S(1)}, bf16[176,256]{1,0:T(8,128)(2,1)S(1)}, u32[]{:S(2)}, u32[]{:S(2)}) collective-permute-start(bf16[176,256]{1,0:T(8,128)(2,1)S(1)} %copy-done.4), channel_id=1, source_target_pairs={{16,0},{24,8},{0,16},{8,24},{17,1},{25,9},{1,17},{9,25},{18,2},{26... | collective-permute-start | bytes 270344 | tf_op jit(solution)/shard_map/ppermute | solution.py:411
  79.4 6.5 %collective-permute-start.9 = (bf16[176,256]{1,0:T(8,128)(2,1)S(1)}, bf16[176,256]{1,0:T(8,128)(2,1)S(1)}, u32[]{:S(2)}, u32[]{:S(2)}) collective-permute-start(bf16[176,256]{1,0:T(8,128)(2,1)S(1)} %copy-done.4), channel_id=1, source_target_pairs={{24,0},{0,8},{8,16},{16,24},{25,1},{1,9},{9,17},{17,25},{26,2},{2,... | collective-permute-start | bytes 270344 | tf_op jit(solution)/shard_map/ppermute | solution.py:411
  87.0 15.4 %all-to-all-start.4 = ((bf16[32,24,128]{2,1,0:T(8,128)(2,1)}), bf16[32,24,128]{2,1,0:T(8,128)(2,1)S(1)}, u32[]{:S(2)}, u32[]{:S(2)}) async-start(bf16[32,24,128]{2,1,0:T(8,128)(2,1)} %shard_map.210), calls=%async_computation.4 | async-start | bytes 393216 | tf_op jit(solution)/shard_map/all_to_all | solution.py:22
where the time goes:
time: 104 us; the launch traced here: 103 us
  blocking collectives  48 us (46%)
  waiting for transfers between devices  23.9 us (23%)
  starting transfers between devices  18.9 us (18%)
  Pallas kernels  9.28 us (9%)
  other arithmetic  1.7 us (2%)
    all_to_all x3, blocking collectives, exchange(): return lax.all_to_all(value, axis, split_axis=0, concat_axis=0, tiled=True)  48 us
    all_to_all x2, waiting for transfers between devices, exchange(): return lax.all_to_all(value, axis, split_axis=0, concat_axis=0, tiled=True)  9.84 us
    all_to_all x2, starting transfers between devices, exchange(): return lax.all_to_all(value, axis, split_axis=0, concat_axis=0, tiled=True)  9.38 us
    ppermute x4, waiting for transfers between devices, piece(): return lax.ppermute(both, ('x', 'c'), pairs)  6.83 us
    ppermute x3, waiting for transfers between devices, one_device(): lax.ppermute(dense_down, 'x', [((i + k) % n_x, i) for i in range(n_x)])  6.49 us
    ppermute x4, starting transfers between devices, piece(): return lax.ppermute(both, ('x', 'c'), pairs)  5.54 us
    pallas_call x1, Pallas kernels, one_device(): call(head_body, [sds((n_tp, seqs, cols), BF), sds((seqs, size), F32), sds...  3.69 us
    ppermute x3, starting transfers between devices, one_device(): lax.ppermute(dense_down, 'x', [((i + k) % n_x, i) for i in range(n_x)])  3.25 us
  transfers between devices with their start and end apart: 12, of which 8 were waited for; matrix products, arithmetic and copies ran while one was open for 2% of the time, Pallas kernels for 0%

commit v1 on v0

--- a/solution.py
+++ b/solution.py
@@ -183,7 +183,7 @@
     n_x = lax.axis_size("x")
     n_blocks = len(rest) // 2
     weights, weights_other = rest[:n_blocks], rest[n_blocks : 2 * n_blocks]
-    core, tp = place_of()
+    _, tp = place_of()
     sources, _, lanes = own.shape
     n_y = out.shape[0]
     hids, cols = weights[0].shape
@@ -198,15 +198,10 @@
     turn = at == row // slots * (pieces * slots) + to // n_slots * slots + row % slots
     turn = turn.astype(F32).astype(BF)
 
-    def expert_rows(ref, which):
-        rows = ref[:, pieces * share :, :].reshape(pieces * n_slots, lanes)
-        rows = dot(turn, rows).astype(BF)
-        start = pl.multiple_of(top + which * pieces * n_slots, 16)
-        for i in range(n_y):
-            out[i, pl.ds(start, pieces * n_slots), :] = rows
-
-    expert_rows(own, core)
-    expert_rows(other, 1 - core)
+    rows = own[:, pieces * share :, :].reshape(pieces * n_slots, lanes)
+    rows = dot(turn, rows).astype(BF)
+    for i in range(n_y):
+        out[i, top:, :] = rows
 
     def columns(ref, which):
         table = ref[...].astype(F32)
@@ -246,38 +241,58 @@
             out[k * halves + t, hids:top, :] = low[:, part]
 
 
-def expert_body(
-    got, gain, gate, up, hidden_out, expert_out, x_mem
-):
+def hidden_body(got, hidden_out, rows_out):
     n_y, _, lanes = got.shape
     hid = hidden_out.shape[0]
-    n_slots, width = x_mem.shape
     top = 2 * hid + 16
-    per_y = width // n_y // lanes
-    square = jnp.zeros((n_slots, 1), F32)
-    for b in range(width // lanes):
-        start = top + b % per_y * n_slots
-        piece = got[b // per_y, start : start + n_slots, :].astype(F32)
-        square = square + jnp.sum(piece * piece, axis=1, keepdims=True)
-    scale = lax.rsqrt(square / width + EPSILON)
-    gains = gain[...].astype(F32)
-    for b in range(width // lanes):
-        start = top + b % per_y * n_slots
-        piece = got[b // per_y, start : start + n_slots, :].astype(F32)
-        part = slice(b * lanes, (b + 1) * lanes)
-        x_mem[:, part] = (piece * scale * gains[b : b + 1, :]).astype(BF)
-
+    width = 2 * n_y * (rows_out.shape[1] // 128) * lanes
     sums = got[0, 0:top, :].astype(F32)
     for i in range(1, n_y):
         sums = sums + got[i, 0:top, :].astype(F32)
+    for i in range(n_y):
+        rows_out[i] = got[i, top:, :]
     factor = lax.rsqrt(sums[2 * hid + 1 : 2 * hid + 2] / width + EPSILON)
     mixing = jax.nn.sigmoid(sums[2 * hid : 2 * hid + 1] * factor)
     dense = silu(sums[:hid] * factor) * (sums[hid : 2 * hid] * factor) * mixing
     hidden_out[...] = dense.astype(BF)
 
+
+def expert_body(mine, theirs, gain, gate, up, expert_out, x_mem):
+    core, _ = place_of()
+    n_y, _, lanes = mine.shape
+    n_slots, width = x_mem.shape
+    per_y = width // n_y // lanes
+    pieces = per_y // 2
+    square = jnp.zeros((n_slots, 1), F32)
+    for i in range(n_y):
+        for h in range(pieces):
+            for ref in (mine, theirs):
+                piece = ref[i, h * n_slots : (h + 1) * n_slots, :].astype(F32)
+                square = square + jnp.sum(piece * piece, axis=1, keepdims=True)
+    scale = lax.rsqrt(square / width + EPSILON)
+    gains = gain[...].astype(F32)
+    for i in range(n_y):
+        for h in range(pieces):
+            here = mine[i, h * n_slots : (h + 1) * n_slots, :].astype(F32)
+            there = theirs[i, h * n_slots : (h + 1) * n_slots, :].astype(F32)
+            for c in range(2):
+                b = i * per_y + c * pieces + h
+                piece = jnp.where(core == c, here, there) * scale * gains[b : b + 1, :]
+                x_mem[:, b * lanes : (b + 1) * lanes] = piece.astype(BF)
     gates = dot(x_mem[...], gate[0])
     ups = dot(x_mem[...], up[0])
     expert_out[...] = (silu(gates) * ups).astype(BF)
+
+
+def fetch_body(source, out, sems):
+    moves = []
+    for i in range(sems.shape[0]):
+        step = source.shape[1] // sems.shape[0]
+        part = pl.ds(i * step, step)
+        moves.append(pltpu.make_async_copy(source.at[0, part], out.at[0, part], sems.at[i]))
+        moves[-1].start()
+    for move in moves:
+        move.wait()
 
 
 def down_body(other, hidden, down, out):
@@ -420,22 +435,31 @@
     )(arrived, resid, routes.T, route_weight.T)
     rows = exchange(outgoing, EP)
 
+    expert_up = call(
+        fetch_body, sds(expert_up.shape, BF), [HBM],
+        [pltpu.SemaphoreType.DMA((4,))],
+    )(pltpu.with_memory_space_constraint(expert_up, pltpu.HBM))
+
     def table(value):
         return value.reshape(width // lanes, lanes)
 
     rows_other = swap_cores(rows)
     sent = call(
-        dense_body, sds((n_y, 2 * hid + 16 + n_c * pieces * n_slots, lanes), BF),
+        dense_body, sds((n_y, 2 * hid + 16 + pieces * n_slots, lanes), BF),
         [VMEM] * (4 + 2 * blocks),
     )(rows, rows_other, table(ffn_gain), table(w_mix), *weights, *weights_other)
     got = exchange(sent, "y")
 
-    hidden, expert_hidden = call(
-        expert_body,
-        [sds((hid, lanes), BF), sds((n_slots, expert_gate.shape[2]), BF)],
-        [VMEM] * 4,
+    hidden, expert_rows = call(
+        hidden_body,
+        [sds((hid, lanes), BF), sds((n_y, pieces * n_slots, lanes), BF)], [VMEM],
+    )(got)
+    rows_there = swap_cores(expert_rows)
+    hidden_other = swap_cores(hidden)
+    expert_hidden = call(
+        expert_body, sds((n_slots, expert_gate.shape[2]), BF), [VMEM] * 5,
         [pltpu.VMEM((n_slots, width), BF)],
-    )(got, table(ffn_gain), expert_gate, expert_up)
+    )(expert_rows, rows_there, table(ffn_gain), expert_gate, expert_up)
 
     def down_half(other):
         return call(
@@ -448,7 +472,7 @@
     keep = down_half(0)
     sent = call(
         pair_body, sds((n_y, pieces * n_slots + n_c * hid, lanes), BF), [VMEM] * 4,
-    )(keep, half, hidden, swap_cores(hidden))
+    )(keep, half, hidden, hidden_other)
     got = exchange(sent, "y")
 
     back = call(

time: 104 us -> 103 us (level)
  blocking collectives: 48 us -> 45 us
  Pallas kernels: 9.28 us -> 10.9 us
    all_to_all x3, blocking collectives: 48 us -> 45 us  [exchange(): return lax.all_to_all(value, axis, split_axis=0, concat_axis=0, tiled=True)]
    pallas_call x2 -> x4, Pallas kernels: 1.66 us -> 3.3 us  [the longest x1 1.58 us: one_device(): call(fetch_body, sds(expert_up.shape, BF), [HBM], [pltpu.SemaphoreType.DM...]
  transfers between devices with their start and end apart: 12 -> 13, of which waited for: 8 -> 8; matrix products, arithmetic and copies ran while one was open for 2% -> 2% of each run, Pallas kernels for 0% -> 2%
where the time goes in v1:
time: 103 us; the launch traced here: 102 us
  blocking collectives  45 us (44%)
  waiting for transfers between devices  23 us (22%)
  starting transfers between devices  19.8 us (19%)
  Pallas kernels  10.9 us (11%)
  other arithmetic  1.7 us (2%)
    all_to_all x3, blocking collectives, exchange(): return lax.all_to_all(value, axis, split_axis=0, concat_axis=0, tiled=True)  45 us
    all_to_all x2, waiting for transfers between devices, exchange(): return lax.all_to_all(value, axis, split_axis=0, concat_axis=0, tiled=True)  9.69 us
    all_to_all x2, starting transfers between devices, exchange(): return lax.all_to_all(value, axis, split_axis=0, concat_axis=0, tiled=True)  9.54 us
    ppermute x4, waiting for transfers between devices, piece(): return lax.ppermute(both, ('x', 'c'), pairs)  6.83 us
    ppermute x3, waiting for transfers between devices, one_device(): lax.ppermute(dense_down, 'x', [((i + k) % n_x, i) for i in range(n_x)])  5.76 us
    ppermute x4, starting transfers between devices, piece(): return lax.ppermute(both, ('x', 'c'), pairs)  5.55 us
    pallas_call x1, Pallas kernels, one_device(): call(head_body, [sds((n_tp, seqs, cols), BF), sds((seqs, size), F32), sds...  3.69 us
    ppermute x3, starting transfers between devices, one_device(): lax.ppermute(dense_down, 'x', [((i + k) % n_x, i) for i in range(n_x)])  3.51 us
  transfers between devices with their start and end apart: 13, of which 8 were waited for; matrix products, arithmetic and copies ran while one was open for 2% of the time, Pallas kernels for 2%

profile of v1, /device:TPU:24, one launch (start us, length us, event | category | flops | bytes accessed | tf_op | source)
XLA Modules:
  0.0 101.9 jit_solution(829820455092442897)
XLA Ops:
  0.6 0.0 copy-start.2
  0.7 0.0 copy-start.6
  0.7 0.0 copy-start.7
  0.7 0.0 copy-start.9
  0.7 0.0 copy-start.10
  0.7 0.0 copy-start.4
  0.7 0.0 copy-start.5
  0.7 3.7 %shard_map.203 = (bf16[8,32,256]{2,1,0:T(8,128)(2,1)S(1)}, f32[32,128]{1,0:T(8,128)S(1)}, f32[32,128]{1,0:T(8,128)S(1)}) custom-call(f32[1,128]{1,0:T(1,128)S(1)} %fusion.3.inverse, bf16[32,2048]{1,0:T(8,128)(2,1)} %resid.3, bf16[16,128]{1,0:T(8,128)(2,1)} %bitcast.18, s32[1,32]{1,0:T(1,128)} %bitcast.19, bf16[1,128]{1,0:T(2,128)(2,1)} %bitcast.20, ...), custom_call_target="tpu_custom_call" | custom-call | tf_op jit(solution)/shard_map/pallas_call | solution.py:396
  4.4 8.5 %all_to_all.25.arrived = bf16[8,32,256]{2,1,0:T(8,128)(2,1)S(1)} all-to-all(bf16[8,32,256]{2,1,0:T(8,128)(2,1)S(1)} %get-tuple-element.10), channel_id=1, replica_groups=mesh['z'=8,'x'=4,'y'=4,'c'=2] {'y','c'}, dimensions={0} | all-to-all | bytes 262144 | tf_op jit(solution)/shard_map/all_to_all | solution.py:22
  12.9 0.0 copy-done.2
  12.9 0.0 copy-done.6
  13.0 0.0 copy-done.7
  13.0 0.5 shard_map.204
  13.5 22.6 %all_to_all.26.own = bf16[32,24,128]{2,1,0:T(8,128)(2,1)S(1)} all-to-all(bf16[32,24,128]{2,1,0:T(8,128)(2,1)S(1)} %get-tuple-element.11), channel_id=1, replica_groups=mesh['z'=8,'x'=4,'y'=4,'c'=2] {'z','x'}, dimensions={0} | all-to-all | bytes 393216 | tf_op jit(solution)/shard_map/all_to_all | solution.py:22
  36.1 0.0 collective-permute-start
  36.1 0.0 copy-done.9
  36.1 0.0 copy-done.10
  36.1 0.7 collective-permute-start.1
  36.8 1.3 %collective-permute-start.2 = (bf16[352,256]{1,0:T(8,128)(2,1)S(1)}, bf16[352,256]{1,0:T(8,128)(2,1)S(1)}, u32[]{:S(2)}, u32[]{:S(2)}) collective-permute-start(bf16[352,256]{1,0:T(8,128)(2,1)S(1)} %pad_maximum_fusion), channel_id=1, source_target_pairs={{8,0},{25,1},{16,8},{1,9},{24,16},{9,17},{0,24},{17,25},{10,2},{27... | collective-permute-start | bytes 540680 | tf_op jit(solution)/shard_map/ppermute | solution.py:421
  38.1 3.6 %collective-permute-start.3 = (bf16[352,256]{1,0:T(8,128)(2,1)S(1)}, bf16[352,256]{1,0:T(8,128)(2,1)S(1)}, u32[]{:S(2)}, u32[]{:S(2)}) collective-permute-start(bf16[352,256]{1,0:T(8,128)(2,1)S(1)} %pad_maximum_fusion), channel_id=1, source_target_pairs={{1,0},{16,1},{9,8},{24,9},{17,16},{0,17},{25,24},{8,25},{3,2},{18,... | collective-permute-start | bytes 540680 | tf_op jit(solution)/shard_map/ppermute | solution.py:421
  41.7 0.0 collective-permute-start.4
  41.7 0.0 collective-permute-done.1.rest_0_
  41.7 1.9 %collective-permute-done.2.rest_1_ = bf16[352,256]{1,0:T(8,128)(2,1)S(1)} collective-permute-done((bf16[352,256]{1,0:T(8,128)(2,1)S(1)}, bf16[352,256]{1,0:T(8,128)(2,1)S(1)}, u32[]{:S(2)}, u32[]{:S(2)}) %collective-permute-start.2) | collective-permute-done | bytes 180256 | tf_op jit(solution)/shard_map/ppermute | solution.py:421
  43.6 2.2 %collective-permute-done.3.rest_2_ = bf16[352,256]{1,0:T(8,128)(2,1)S(1)} collective-permute-done((bf16[352,256]{1,0:T(8,128)(2,1)S(1)}, bf16[352,256]{1,0:T(8,128)(2,1)S(1)}, u32[]{:S(2)}, u32[]{:S(2)}) %collective-permute-start.3) | collective-permute-done | bytes 180256 | tf_op jit(solution)/shard_map/ppermute | solution.py:421
  45.8 2.7 %collective-permute-done.4.rest_3_ = bf16[352,256]{1,0:T(8,128)(2,1)S(1)} collective-permute-done((bf16[352,256]{1,0:T(8,128)(2,1)S(1)}, bf16[352,256]{1,0:T(8,128)(2,1)S(1)}, u32[]{:S(2)}, u32[]{:S(2)}) %collective-permute-start.4) | collective-permute-done | bytes 180256 | tf_op jit(solution)/shard_map/ppermute | solution.py:421
  48.5 0.0 collective-permute-done.other
  48.5 0.0 copy-done.4
  48.5 0.0 copy-done.5
  48.5 0.6 shard_map.205
  49.1 13.8 %all_to_all.27.got = bf16[4,624,128]{2,1,0:T(8,128)(2,1)S(1)} all-to-all(bf16[4,624,128]{2,1,0:T(8,128)(2,1)S(1)} %shard_map.205), channel_id=1, replica_groups=mesh['z'=8,'x'=4,'y'=4,'c'=2] {'y'}, dimensions={0} | all-to-all | bytes 1277952 | tf_op jit(solution)/shard_map/all_to_all | solution.py:22
  62.9 0.1 shard_map.206
  63.0 0.0 copy-start.1
  63.0 0.6 collective-permute-start.5
  63.6 1.6 %shard_map.207.up = bf16[1,2048,512]{2,1,0:T(8,128)(2,1)S(1)} custom-call(bf16[1,2048,512]{2,1,0:T(8,128)(2,1)} %source.1), custom_call_target="tpu_custom_call" | custom-call | tf_op jit(solution)/shard_map/pallas_call | solution.py:438
  65.2 0.0 copy-start
  65.2 0.0 collective-permute-done.5.theirs
  65.2 0.0 copy-done.1
  65.2 1.1 %shard_map.208.hidden = bf16[128,512]{1,0:T(8,128)(2,1)S(1)} custom-call(bf16[4,256,128]{2,1,0:T(8,128)(2,1)S(1)} %get-tuple-element.12.mine, bf16[4,256,128]{2,1,0:T(8,128)(2,1)S(1)} %collective-permute-done.5.theirs, bf16[16,128]{1,0:T(8,128)(2,1)S(1)} %bitcast.11, bf16[1,2048,512]{2,1,0:T(8,128)(2,1)S(1)} %copy-done.1, ...), custom_call_target="tpu_custom_call" | custom-call | tf_op jit(solution)/shard_map/pallas_call | solution.py:459
  66.3 0.5 copy-done
  66.8 0.3 shard_map.210
  67.1 0.3 collective-permute-start.6
  67.4 0.0 copy-start.3
  67.4 0.3 collective-permute-start.7
  67.7 0.3 shard_map.209.keep
  68.1 0.0 copy-start.8
  68.1 0.7 collective-permute-done.7.hidden_other
  68.8 0.0 collective-permute-done.6.got
  68.8 0.9 shard_map.211
  69.7 5.5 %all-to-all-start.3 = ((bf16[4,608,128]{2,1,0:T(8,128)(2,1)}), bf16[4,608,128]{2,1,0:T(8,128)(2,1)S(1)}, u32[]{:S(2)}, u32[]{:S(2)}) async-start(bf16[4,608,128]{2,1,0:T(8,128)(2,1)} %shard_map.211), calls=%async_computation.3 | async-start | bytes 1245184 | tf_op jit(solution)/shard_map/all_to_all | solution.py:22
  75.3 0.0 copy-done.3
  75.3 1.0 collective-permute-start.10
  76.3 2.2 %collective-permute-start.8 = (bf16[176,256]{1,0:T(8,128)(2,1)S(1)}, bf16[176,256]{1,0:T(8,128)(2,1)S(1)}, u32[]{:S(2)}, u32[]{:S(2)}) collective-permute-start(bf16[176,256]{1,0:T(8,128)(2,1)S(1)} %copy-done.3), channel_id=1, source_target_pairs={{8,0},{16,8},{24,16},{0,24},{9,1},{17,9},{25,17},{1,25},{10,2},{18... | collective-permute-start | bytes 270344 | tf_op jit(solution)/shard_map/ppermute | solution.py:426
  78.5 0.3 collective-permute-start.9
  78.8 2.2 %collective-permute-done.10.rest_3_ = bf16[176,256]{1,0:T(8,128)(2,1)S(1)} collective-permute-done((bf16[176,256]{1,0:T(8,128)(2,1)S(1)}, bf16[176,256]{1,0:T(8,128)(2,1)S(1)}, u32[]{:S(2)}, u32[]{:S(2)}) %collective-permute-start.10) | collective-permute-done | bytes 90144 | tf_op jit(solution)/shard_map/ppermute | solution.py:426
  81.0 1.3 %collective-permute-done.8.rest_1_ = bf16[176,256]{1,0:T(8,128)(2,1)S(1)} collective-permute-done((bf16[176,256]{1,0:T(8,128)(2,1)S(1)}, bf16[176,256]{1,0:T(8,128)(2,1)S(1)}, u32[]{:S(2)}, u32[]{:S(2)}) %collective-permute-start.8) | collective-permute-done | bytes 90144 | tf_op jit(solution)/shard_map/ppermute | solution.py:426
  82.3 2.2 %collective-permute-done.9.rest_2_ = bf16[176,256]{1,0:T(8,128)(2,1)S(1)} collective-permute-done((bf16[176,256]{1,0:T(8,128)(2,1)S(1)}, bf16[176,256]{1,0:T(8,128)(2,1)S(1)}, u32[]{:S(2)}, u32[]{:S(2)}) %collective-permute-start.9) | collective-permute-done | bytes 90144 | tf_op jit(solution)/shard_map/ppermute | solution.py:426
  84.5 0.0 all-to-all-done.3.got
  84.6 1.1 %shard_map.212 = bf16[32,24,128]{2,1,0:T(8,128)(2,1)} custom-call(bf16[4,608,128]{2,1,0:T(8,128)(2,1)S(1)} %all-to-all-done.3.got, bf16[176,256]{1,0:T(8,128)(2,1)S(1)} %copy-done.3, bf16[176,256]{1,0:T(8,128)(2,1)S(1)} %collective-permute-done.8.rest_1_, bf16[176,256]{1,0:T(8,128)(2,1)S(1)} %collective-permute-done.9.rest_2_, ...), custom_call_target="tpu_custom_call" | custom-call | tf_op jit(solution)/shard_map/pallas_call | solution.py:478
  85.6 4.0 %all-to-all-start.4 = ((bf16[32,24,128]{2,1,0:T(8,128)(2,1)}), bf16[32,24,128]{2,1,0:T(8,128)(2,1)S(1)}, u32[]{:S(2)}, u32[]{:S(2)}) async-start(bf16[32,24,128]{2,1,0:T(8,128)(2,1)} %shard_map.212), calls=%async_computation.4 | async-start | bytes 393216 | tf_op jit(solution)/shard_map/all_to_all | solution.py:22
  89.7 0.0 copy-done.8
  89.7 1.7 %multiply_add_fusion = f32[32,1,128,128]{3,2,1,0:T(8,128)} fusion(f32[32,1,128,128]{3,2,1,0:T(8,128)S(1)} %copy-done.8, f32[32,128]{1,0:T(8,128)S(1)} %get-tuple-element.17, f32[32,128]{1,0:T(8,128)S(1)} %get-tuple-element.16, f32[]{:T(128)S(6)} %sub.7), kind=kLoop, calls=%fused_computation | loop fusion | flops 1572864 | bytes 4227076 | tf_op jit(solution)/shard_map/add | solution.py:409
  91.4 9.7 %all-to-all-done.4.back = bf16[32,24,128]{2,1,0:T(8,128)(2,1)S(1)} async-done(((bf16[32,24,128]{2,1,0:T(8,128)(2,1)}), bf16[32,24,128]{2,1,0:T(8,128)(2,1)S(1)}, u32[]{:S(2)}, u32[]{:S(2)}) %all-to-all-start.4) | async-done | bytes 196640 | tf_op jit(solution)/shard_map/all_to_all | solution.py:22
  101.1 0.8 shard_map.213
  (2 shorter events, 0.0 us)
Async XLA Ops:
  0.6 12.3 %copy-start.2 = (bf16[32,2048]{1,0:T(8,128)(2,1)S(1)}, bf16[32,2048]{1,0:T(8,128)(2,1)}, u32[]{:S(2)}) copy-start(bf16[32,2048]{1,0:T(8,128)(2,1)} %resid.3) | copy-start | bytes 393220
  0.7 12.3 %copy-start.6 = (s32[32,2]{0,1:T(2,128)S(1)}, s32[32,2]{0,1:T(2,128)}, u32[]{:S(2)}) copy-start(s32[32,2]{0,1:T(2,128)} %param.35) | copy-start | bytes 772
  0.7 12.3 %copy-start.7 = (bf16[32,2]{0,1:T(2,128)(2,1)S(1)}, bf16[32,2]{0,1:T(2,128)(2,1)}, u32[]{:S(2)}) copy-start(bf16[32,2]{0,1:T(2,128)(2,1)} %param.36) | copy-start | bytes 388
  0.7 35.4 %copy-start.9 = (bf16[256,176]{0,1:T(8,128)(2,1)S(1)}, bf16[256,176]{0,1:T(8,128)(2,1)}, u32[]{:S(2)}) copy-start(bf16[256,176]{0,1:T(8,128)(2,1)} %param.33) | copy-start | bytes 270340
  0.7 35.4 %copy-start.10 = (bf16[256,176]{0,1:T(8,128)(2,1)S(1)}, bf16[256,176]{0,1:T(8,128)(2,1)}, u32[]{:S(2)}) copy-start(bf16[256,176]{0,1:T(8,128)(2,1)} %param.32) | copy-start | bytes 270340
  0.7 47.8 %copy-start.4 = (bf16[2048]{0:T(1024)(128)(2,1)S(1)}, bf16[2048]{0:T(1024)(128)(2,1)}, u32[]{:S(2)}) copy-start(bf16[2048]{0:T(1024)(128)(2,1)} %param.30) | copy-start | bytes 12292
  0.7 47.8 %copy-start.5 = (bf16[2048]{0:T(1024)(128)(2,1)S(1)}, bf16[2048]{0:T(1024)(128)(2,1)}, u32[]{:S(2)}) copy-start(bf16[2048]{0:T(1024)(128)(2,1)} %param.31) | copy-start | bytes 12292
  36.1 12.4 %collective-permute-start = (bf16[32,24,128]{2,1,0:T(8,128)(2,1)S(1)}, bf16[32,24,128]{2,1,0:T(8,128)(2,1)S(1)}, u32[]{:S(2)}, u32[]{:S(2)}) collective-permute-start(bf16[32,24,128]{2,1,0:T(8,128)(2,1)S(1)} %all_to_all.26.own), channel_id=1, source_target_pairs={{0,1},{1,0},{2,3},{3,2},{4,5},{5,4},{6,7},{7,6},{8,9},{9,8},{10,11... | collective-permute-start | bytes 589832 | tf_op jit(solution)/shard_map/ppermute | solution.py:26
  36.1 5.6 %collective-permute-start.1 = (bf16[352,256]{1,0:T(8,128)(2,1)S(1)}, bf16[352,256]{1,0:T(8,128)(2,1)S(1)}, u32[]{:S(2)}, u32[]{:S(2)}) collective-permute-start(bf16[352,256]{1,0:T(8,128)(2,1)S(1)} %pad_maximum_fusion), channel_id=1, source_target_pairs={{0,0},{17,1},{8,8},{25,9},{16,16},{1,17},{24,24},{9,25},{2,2},{19,... | collective-permute-start | bytes 540680 | tf_op jit(solution)/shard_map/ppermute | solution.py:421
  36.8 6.8 %collective-permute-start.2 = (bf16[352,256]{1,0:T(8,128)(2,1)S(1)}, bf16[352,256]{1,0:T(8,128)(2,1)S(1)}, u32[]{:S(2)}, u32[]{:S(2)}) collective-permute-start(bf16[352,256]{1,0:T(8,128)(2,1)S(1)} %pad_maximum_fusion), channel_id=1, source_target_pairs={{8,0},{25,1},{16,8},{1,9},{24,16},{9,17},{0,24},{17,25},{10,2},{27... | collective-permute-start | bytes 540680 | tf_op jit(solution)/shard_map/ppermute | solution.py:421
  38.1 7.7 %collective-permute-start.3 = (bf16[352,256]{1,0:T(8,128)(2,1)S(1)}, bf16[352,256]{1,0:T(8,128)(2,1)S(1)}, u32[]{:S(2)}, u32[]{:S(2)}) collective-permute-start(bf16[352,256]{1,0:T(8,128)(2,1)S(1)} %pad_maximum_fusion), channel_id=1, source_target_pairs={{1,0},{16,1},{9,8},{24,9},{17,16},{0,17},{25,24},{8,25},{3,2},{18,... | collective-permute-start | bytes 540680 | tf_op jit(solution)/shard_map/ppermute | solution.py:421
  41.7 6.8 %collective-permute-start.4 = (bf16[352,256]{1,0:T(8,128)(2,1)S(1)}, bf16[352,256]{1,0:T(8,128)(2,1)S(1)}, u32[]{:S(2)}, u32[]{:S(2)}) collective-permute-start(bf16[352,256]{1,0:T(8,128)(2,1)S(1)} %pad_maximum_fusion), channel_id=1, source_target_pairs={{9,0},{24,1},{17,8},{0,9},{25,16},{8,17},{1,24},{16,25},{11,2},{26... | collective-permute-start | bytes 540680 | tf_op jit(solution)/shard_map/ppermute | solution.py:421
  63.0 2.2 %copy-start.1 = (bf16[1,2048,512]{2,1,0:T(8,128)(2,1)S(1)}, bf16[1,2048,512]{2,1,0:T(8,128)(2,1)}, u32[]{:S(2)}) copy-start(bf16[1,2048,512]{2,1,0:T(8,128)(2,1)} %gate.1) | copy-start | bytes 6291460
  63.0 2.2 %collective-permute-start.5 = (bf16[4,256,128]{2,1,0:T(8,128)(2,1)S(1)}, bf16[4,256,128]{2,1,0:T(8,128)(2,1)S(1)}, u32[]{:S(2)}, u32[]{:S(2)}) collective-permute-start(bf16[4,256,128]{2,1,0:T(8,128)(2,1)S(1)} %get-tuple-element.12.mine), channel_id=1, source_target_pairs={{0,1},{1,0},{2,3},{3,2},{4,5},{5,4},{6,7},{7,6},{8,9},{9,8},{10,11... | collective-permute-start | bytes 786440 | tf_op jit(solution)/shard_map/ppermute | solution.py:26
  65.2 1.6 %copy-start = (bf16[1,512,2048]{2,1,0:T(8,128)(2,1)S(1)}, bf16[1,512,2048]{2,1,0:T(8,128)(2,1)}, u32[]{:S(2)}) copy-start(bf16[1,512,2048]{2,1,0:T(8,128)(2,1)} %down.3) | copy-start | bytes 6291460
  67.1 1.7 %collective-permute-start.6 = (bf16[4,128,256]{2,1,0:T(8,128)(2,1)S(1)}, bf16[4,128,256]{2,1,0:T(8,128)(2,1)S(1)}, u32[]{:S(2)}, u32[]{:S(2)}) collective-permute-start(bf16[4,128,256]{2,1,0:T(8,128)(2,1)S(1)} %shard_map.210), channel_id=1, source_target_pairs={{0,1},{1,0},{2,3},{3,2},{4,5},{5,4},{6,7},{7,6},{8,9},{9,8},{10,11... | collective-permute-start | bytes 786440 | tf_op jit(solution)/shard_map/ppermute | solution.py:26
  67.4 7.9 %copy-start.3 = (bf16[176,256]{1,0:T(8,128)(2,1)S(1)}, bf16[176,256]{1,0:T(8,128)(2,1)}, u32[]{:S(2)}) copy-start(bf16[176,256]{1,0:T(8,128)(2,1)} %rest_0_.1) | copy-start | bytes 270340
  67.4 1.4 %collective-permute-start.7 = (bf16[176,128]{1,0:T(8,128)(2,1)S(1)}, bf16[176,128]{1,0:T(8,128)(2,1)S(1)}, u32[]{:S(2)}, u32[]{:S(2)}) collective-permute-start(bf16[176,128]{1,0:T(8,128)(2,1)S(1)} %get-tuple-element.13.hidden), channel_id=1, source_target_pairs={{0,1},{1,0},{2,3},{3,2},{4,5},{5,4},{6,7},{7,6},{8,9},{9,8},{10,11... | collective-permute-start | bytes 135176 | tf_op jit(solution)/shard_map/ppermute | solution.py:26
  68.1 21.6 %copy-start.8 = (f32[32,1,128,128]{3,2,1,0:T(8,128)S(1)}, f32[32,1,128,128]{3,2,1,0:T(8,128)}, u32[]{:S(2)}) copy-start(f32[32,1,128,128]{3,2,1,0:T(8,128)} %param.28) | copy-start | bytes 6291460
  69.7 14.8 %all-to-all-start.3 = ((bf16[4,608,128]{2,1,0:T(8,128)(2,1)}), bf16[4,608,128]{2,1,0:T(8,128)(2,1)S(1)}, u32[]{:S(2)}, u32[]{:S(2)}) async-start(bf16[4,608,128]{2,1,0:T(8,128)(2,1)} %shard_map.211), calls=%async_computation.3 | async-start | bytes 1245184 | tf_op jit(solution)/shard_map/all_to_all | solution.py:22
  75.3 5.7 %collective-permute-start.10 = (bf16[176,256]{1,0:T(8,128)(2,1)S(1)}, bf16[176,256]{1,0:T(8,128)(2,1)S(1)}, u32[]{:S(2)}, u32[]{:S(2)}) collective-permute-start(bf16[176,256]{1,0:T(8,128)(2,1)S(1)} %copy-done.3), channel_id=1, source_target_pairs={{24,0},{0,8},{8,16},{16,24},{25,1},{1,9},{9,17},{17,25},{26,2},{2,... | collective-permute-start | bytes 270344 | tf_op jit(solution)/shard_map/ppermute | solution.py:426
  76.3 6.0 %collective-permute-start.8 = (bf16[176,256]{1,0:T(8,128)(2,1)S(1)}, bf16[176,256]{1,0:T(8,128)(2,1)S(1)}, u32[]{:S(2)}, u32[]{:S(2)}) collective-permute-start(bf16[176,256]{1,0:T(8,128)(2,1)S(1)} %copy-done.3), channel_id=1, source_target_pairs={{8,0},{16,8},{24,16},{0,24},{9,1},{17,9},{25,17},{1,25},{10,2},{18... | collective-permute-start | bytes 270344 | tf_op jit(solution)/shard_map/ppermute | solution.py:426
  78.5 6.0 %collective-permute-start.9 = (bf16[176,256]{1,0:T(8,128)(2,1)S(1)}, bf16[176,256]{1,0:T(8,128)(2,1)S(1)}, u32[]{:S(2)}, u32[]{:S(2)}) collective-permute-start(bf16[176,256]{1,0:T(8,128)(2,1)S(1)} %copy-done.3), channel_id=1, source_target_pairs={{16,0},{24,8},{0,16},{8,24},{17,1},{25,9},{1,17},{9,25},{18,2},{26... | collective-permute-start | bytes 270344 | tf_op jit(solution)/shard_map/ppermute | solution.py:426
  85.6 15.4 %all-to-all-start.4 = ((bf16[32,24,128]{2,1,0:T(8,128)(2,1)}), bf16[32,24,128]{2,1,0:T(8,128)(2,1)S(1)}, u32[]{:S(2)}, u32[]{:S(2)}) async-start(bf16[32,24,128]{2,1,0:T(8,128)(2,1)} %shard_map.212), calls=%async_computation.4 | async-start | bytes 393216 | tf_op jit(solution)/shard_map/all_to_all | solution.py:22
